TPU v7x, 32 devices: a whole 2x2x4 slice. The times are simulated.
32 devices in a mesh: grp: 2 (over y), tp: 4 (over z), dp: 4 (over x, core).
Axes of the slice: x: 2, y: 2, z: 4, core: 2. Of those that a mesh axis runs over, the one named last changes fastest.
Arguments:
- skip_path_activations: bfloat16 [128, 8, 4096], P('grp', None, 'dp'), parts along dimension 0
- novel_lengths_per_sequence: int32 [128], P(('grp', 'dp')), parts along dimension 0, may hold values from 1 to 8, 256 in all
- input_normalizer_scales: bfloat16 [2, 4096], P(None, 'dp'), may hold values from 0.099609375 to 1.8984375
- question_projector: bfloat16 [2, 4096, 2048], P(None, 'dp', 'tp'), may hold values from -0.09375 to 0.09375
- lookup_projector: bfloat16 [2, 4096, 2048], P(None, 'dp', 'tp'), may hold values from -0.09375 to 0.09375
- payload_projector: bfloat16 [2, 4096, 4096], P(None, 'dp', 'tp'), may hold values from -0.09375 to 0.09375
- emitted_valve_projector: bfloat16 [2, 4096, 4096], P(None, 'dp', 'tp'), may hold values from -0.09375 to 0.09375
- keeping_valve_projector: bfloat16 [2, 4096, 2048], P(None, 'dp', 'tp'), may hold values from -0.09375 to 0.09375
- keeping_valve_shift: float32 [2, 2048], P(None, 'tp'), may hold values from -3 to 6
- additional_dwindle_exponent: float32 [128, 8, 16], P(('grp', 'dp'), None, 'tp'), parts along dimension 0, may hold values from -0.7 to 0
- headwise_normalizer_scales: bfloat16 [2, 256], replicated, may hold values from 0.099609375 to 1.8984375
- closing_projector: bfloat16 [2, 4096, 4096], P(None, 'tp', 'dp'), may hold values from -0.1875 to 0.1875
- earlier_recurrence_grid: float32 [2, 128, 16, 128, 256], P(None, ('grp', 'dp'), 'tp'), parts along dimension 1, may hold values from -6 to 6
Outputs:
- stream_out: bfloat16 [128, 8, 4096], P('grp', None, 'dp'), parts along dimension 0
- state_out: float32 [2, 128, 16, 128, 256], P(None, ('grp', 'dp'), 'tp'), parts along dimension 1
There are 2 independent parts, one for each index of `grp`. A program takes and returns all parts, laid end to end along the dimension named above; an argument that names none is the same for every part. Nothing has to cross between parts.
Inputs may be any that keep to these rules, and one draw needn't show every extreme that they name: `novel_lengths_per_sequence`: each sequence has 1 to 8 live token slots, the first ones; some sequence has 8. In each group the live slots of its 64 sequences add up to half of 64 times 8.
All inputs are finite; a program needn't handle non-finite values.
Results may differ from a plain program's by a relative error of at most 0.024.
Values may be sent and summed in bfloat16 or wider, within the bound.
A program may use at most 128 MiB of HBM per device.

v0:
```python
import jax
import jax.numpy as jnp
from jax import lax
from jax.sharding import PartitionSpec as P

LAYERS = 2


EPS = 1e-06
TAU = 16.0


def scaled_rms(values_f, gain):
    return (
        values_f
        * lax.rsqrt(jnp.mean(values_f * values_f, axis=-1, keepdims=True) + EPS)
        * gain.astype(jnp.float32)
    )


def round_trip(values_f):
    return lax.optimization_barrier(values_f.astype(jnp.bfloat16)).astype(jnp.float32)


def advance(query_rows, key_rows, value_rows, fade_log_amount, carried):
    steps_n = query_rows.shape[1]
    cumulative = jnp.cumsum(fade_log_amount, axis=1)
    spread = cumulative[:, :, None] - cumulative[:, None, :]
    causal = jnp.tril(jnp.ones((steps_n, steps_n), dtype=bool))
    decay_mat = jnp.exp(jnp.where(causal[None, :, :, None, None], spread, -jnp.inf))
    scores = jnp.einsum(
        "sihd,sjhd,sijhd->shij", query_rows, key_rows, decay_mat, precision=lax.Precision.HIGHEST
    )
    within = jnp.einsum("shij,sjhv->sihv", scores, value_rows, precision=lax.Precision.HIGHEST)
    carried_part = jnp.einsum(
        "sihd,shdv->sihv",
        query_rows * jnp.exp(cumulative),
        carried,
        precision=lax.Precision.HIGHEST,
    )
    final_log = cumulative[:, -1]
    weighted = key_rows * jnp.exp(final_log[:, None] - cumulative)
    updated = jnp.exp(final_log)[..., None] * carried + jnp.einsum(
        "sjhd,sjhv->shdv", weighted, value_rows, precision=lax.Precision.HIGHEST
    )
    return (within + carried_part, updated)


def shards(
    skip_path_activations,
    novel_lengths_per_sequence,
    input_normalizer_scales,
    question_projector,
    lookup_projector,
    payload_projector,
    emitted_valve_projector,
    keeping_valve_projector,
    keeping_valve_shift,
    additional_dwindle_exponent,
    headwise_normalizer_scales,
    closing_projector,
    earlier_recurrence_grid,
):
    number_of_streams, number_of_iterations, shard_breadth = skip_path_activations.shape
    number_of_lines = number_of_streams * number_of_iterations
    local_seqs = novel_lengths_per_sequence.shape[0]
    local_rows = local_seqs * number_of_iterations
    existing_attender_list = additional_dwindle_exponent.shape[2]
    key_dim = earlier_recurrence_grid.shape[3]
    value_dim = earlier_recurrence_grid.shape[4]
    key_cols = existing_attender_list * key_dim
    value_cols = existing_attender_list * value_dim
    full_width = shard_breadth * lax.axis_size("dp")
    ongoing = skip_path_activations.reshape(number_of_lines, shard_breadth)
    live_entry_indicator = (
        lax.broadcasted_iota(jnp.int32, (local_seqs, number_of_iterations), 1)
        < novel_lengths_per_sequence[:, None]
    ).astype(jnp.float32)
    new_states = []
    for block_index in range(LAYERS):
        stream_f = ongoing.astype(jnp.float32)
        square_sum = lax.psum(jnp.sum(stream_f * stream_f, axis=1), "dp")
        normed = (
            stream_f
            * lax.rsqrt(square_sum / full_width + EPS)[:, None]
            * input_normalizer_scales[block_index].astype(jnp.float32)
        ).astype(jnp.bfloat16)
        matrices = (
            question_projector[block_index],
            lookup_projector[block_index],
            payload_projector[block_index],
            emitted_valve_projector[block_index],
            keeping_valve_projector[block_index],
        )
        summed = lax.psum_scatter(
            jnp.concatenate(
                [
                    jnp.dot(normed, matrix, preferred_element_type=jnp.float32)
                    for matrix in matrices
                ],
                axis=1,
            ).astype(jnp.bfloat16),
            "dp",
            scatter_dimension=0,
            tiled=True,
        ).astype(jnp.float32)
        query_rows = round_trip(summed[:, :key_cols]) * key_dim ** (-0.5)
        key_rows = round_trip(summed[:, key_cols : 2 * key_cols])
        value_rows = round_trip(summed[:, 2 * key_cols : 2 * key_cols + value_cols])
        gate_rows = round_trip(summed[:, 2 * key_cols + value_cols : 2 * key_cols + 2 * value_cols])
        logits = summed[:, 2 * key_cols + 2 * value_cols :]
        fade_log_amount = (
            jax.nn.log_sigmoid(logits + keeping_valve_shift[block_index]) / TAU
        ).reshape(local_seqs, number_of_iterations, existing_attender_list, key_dim)
        fade_log_amount = (
            fade_log_amount + additional_dwindle_exponent[..., None]
        ) * live_entry_indicator[:, :, None, None]
        key_rows = (
            key_rows.reshape(local_seqs, number_of_iterations, existing_attender_list, key_dim)
            * live_entry_indicator[:, :, None, None]
        )
        output, updated = advance(
            query_rows.reshape(local_seqs, number_of_iterations, existing_attender_list, key_dim),
            key_rows,
            value_rows.reshape(local_seqs, number_of_iterations, existing_attender_list, value_dim),
            fade_log_amount,
            earlier_recurrence_grid[block_index],
        )
        new_states.append(updated)
        normed_out = scaled_rms(output, headwise_normalizer_scales[block_index]).reshape(
            local_rows, value_cols
        )
        gated_rows = (
            normed_out * jax.nn.silu(gate_rows) * live_entry_indicator.reshape(local_rows, 1)
        ).astype(jnp.bfloat16)
        out_matrix = closing_projector[block_index]
        partial_value = jnp.dot(
            lax.all_gather(gated_rows, "dp", axis=0, tiled=True),
            out_matrix,
            preferred_element_type=jnp.float32,
        )
        head_total = lax.psum(partial_value.astype(jnp.bfloat16), "tp").astype(jnp.float32)
        ongoing = (ongoing.astype(jnp.float32) + head_total).astype(jnp.bfloat16)
    return (
        ongoing.reshape(number_of_streams, number_of_iterations, shard_breadth),
        jnp.stack(new_states, axis=0),
    )


def solution(mesh):
    in_specs = (
        P("grp", None, "dp"),
        P(("grp", "dp")),
        P(None, "dp"),
        P(None, "dp", "tp"),
        P(None, "dp", "tp"),
        P(None, "dp", "tp"),
        P(None, "dp", "tp"),
        P(None, "dp", "tp"),
        P(None, "tp"),
        P(("grp", "dp"), None, "tp"),
        P(),
        P(None, "tp", "dp"),
        P(None, ("grp", "dp"), "tp", None, None),
    )
    out_specs = (P("grp", None, "dp"), P(None, ("grp", "dp"), "tp", None, None))
    return jax.shard_map(shards, mesh=mesh, in_specs=in_specs, out_specs=out_specs, check_vma=False)
```

profile of v0, /device:TPU:0, one launch (start us, length us, event | category | flops | bytes accessed | tf_op | source)
XLA Modules:
  0.0 320.1 jit_solution(2252554068193060623)
XLA Ops:
  9.6 8.4 %psum.28 = f32[512]{0:T(512)S(1)} all-reduce(f32[512]{0:T(512)S(1)} %reduce_sum.39), channel_id=1, replica_groups=mesh['grp'=2,'tp'=4,'dp'=4] {'dp'}, use_global_device_ids=true, to_apply=%region_1.0 | all-reduce | flops 512 | bytes 4096 | tf_op jit(solution)/shard_map/psum | solution.py:82
  18.1 2.5 convolution_convert_fusion.4
  20.8 2.1 convolution_convert_fusion.5
  24.7 4.0 %fusion.42 = bf16[512,3584]{1,0:T(8,128)(2,1)} fusion(bf16[512,3584]{1,0:T(8,128)(2,1)} %constant_dynamic-update-slice_fusion, bf16[2,1024,1024]{2,1,0:T(8,128)(2,1)} %param.18, bf16[64,8,1024]{2,1,0:T(8,128)(2,1)S(1)} %copy-done, f32[1024]{0:T(1024)S(1)} %bitcast.225, f32[64,8]{1,0:T(8,128)S(1)} %mul.190), kind=kOutput, calls=%fused_computation.53 | convolution fusion | flops 1076363264 | bytes 4200448 | tf_op jit(solution)/shard_map/dot_general | solution.py:98
  28.7 2.3 fusion.48
  34.1 40.2 %reduce-scatter.3.cloned.1.call-done = bf16[128,3584]{1,0:T(8,128)(2,1)} async-done(((bf16[512,3584]{1,0:T(8,128)(2,1)}), bf16[128,3584]{1,0:T(8,128)(2,1)}) %reduce-scatter.3.cloned.1.call-update) | async-done | bytes 917520 | tf_op jit(solution)/shard_map/reduce_scatter | solution.py:95
  80.5 6.6 %multiply_reduce_fusion.1 = (f32[16,8,4]{1,2,0:T(4,128)S(1)}, f32[16,8,4,256]{3,1,2,0:T(8,128)S(1)}) fusion(f32[16,8,4,256]{3,1,2,0:T(8,128)S(1)} %convolution_bitcast_fusion.1, f32[2,16,4,128,256]{4,3,2,1,0:T(8,128)} %param.25, f32[16,8,4,128]{3,1,2,0:T(8,128)S(1)} %reduce_window_sum.17, bf16[128,512]{1,0:T(8,128)(2,1)S(1)} %get-tuple-element.9), kind=kOutput, calls=%fused_computation.111 | convolution fusion | flops 201915904 | bytes 9832448 | tf_op jit(solution)/shard_map/sihd,shdv->sihv/dot_general | solution.py:35
  88.4 16.6 %all-gather.3.cloned.1.call-done = bf16[512,1024]{1,0:T(8,128)(2,1)} async-done(((bf16[128,1024]{1,0:T(8,128)(2,1)}), bf16[512,1024]{1,0:T(8,128)(2,1)}) %all-gather.3.cloned.1.call-update) | async-done | bytes 1048592 | tf_op jit(solution)/shard_map/all_gather | solution.py:138
  105.0 4.1 %fusion.51 = bf16[512,1024]{1,0:T(8,128)(2,1)} fusion(bf16[512,1024]{1,0:T(8,128)(2,1)} %all-gather.3.cloned.1.call-done, bf16[2,1024,1024]{2,1,0:T(8,128)(2,1)} %param.24), kind=kOutput, calls=%fused_computation.56 | convolution fusion | flops 1074266112 | bytes 4194304 | tf_op jit(solution)/shard_map/dot_general | solution.py:137
  109.2 52.0 %all-reduce.3.cloned.1.call-done = bf16[512,1024]{1,0:T(8,128)(2,1)} async-done(((bf16[512,1024]{1,0:T(8,128)(2,1)}), bf16[512,1024]{1,0:T(8,128)(2,1)}) %all-reduce.3.cloned.1.call-update) | async-done | bytes 1048592 | tf_op jit(solution)/shard_map/psum | solution.py:142
  163.0 6.8 %psum.30 = f32[512]{0:T(512)S(1)} all-reduce(f32[512]{0:T(512)S(1)} %fusion.10), channel_id=1, replica_groups=mesh['grp'=2,'tp'=4,'dp'=4] {'dp'}, use_global_device_ids=true, to_apply=%region_7.8 | all-reduce | flops 512 | bytes 4096 | tf_op jit(solution)/shard_map/psum | solution.py:82
  174.4 2.2 fusion.57
  176.7 2.2 fusion.63
  180.5 39.7 %reduce-scatter.5.cloned.1.call-done = bf16[128,3584]{1,0:T(8,128)(2,1)} async-done(((bf16[512,3584]{1,0:T(8,128)(2,1)}), bf16[128,3584]{1,0:T(8,128)(2,1)}) %reduce-scatter.5.cloned.1.call-update) | async-done | bytes 917520 | tf_op jit(solution)/shard_map/reduce_scatter | solution.py:95
  221.9 1.8 fusion.151
  223.7 1.9 fusion.122
  229.6 6.6 %multiply_reduce_fusion = (f32[16,8,4]{1,2,0:T(4,128)S(1)}, f32[16,8,4,256]{3,1,2,0:T(8,128)S(1)}) fusion(f32[16,8,4,256]{3,1,2,0:T(8,128)S(1)} %convolution_bitcast_fusion, f32[2,16,4,128,256]{4,3,2,1,0:T(8,128)} %param.25, f32[16,8,4,128]{3,1,2,0:T(8,128)S(1)} %reduce_window_sum.18, bf16[128,512]{1,0:T(8,128)(2,1)S(1)} %get-tuple-element.5), kind=kOutput, calls=%fused_computation.109 | convolution fusion | flops 201915904 | bytes 9832448 | tf_op jit(solution)/shard_map/sihd,shdv->sihv/dot_general | solution.py:35
  237.7 9.3 %fusion.7 = f32[1,16,4,128,256]{4,3,2,1,0:T(8,128)} fusion(f32[2,16,4,128,256]{4,3,2,1,0:T(8,128)} %param.25, f32[16,4,128]{2,1,0:T(4,128)S(1)} %exp.55, bf16[16,8,4,256]{3,1,2,0:T(8,128)(2,1)S(1)} %bitcast.209, f32[16,8,4,128]{3,1,2,0:T(8,128)S(1)} %reduce_window_sum.17, bf16[128,512]{1,0:T(8,128)(2,1)S(1)} %get-tuple-element.8, ...), kind=kOutput, calls=%fused_computation.10 | convolution fusion | flops 205783040 | bytes 17498624 | tf_op jit(solution)/shard_map/sjhd,sjhv->shdv/dot_general | solution.py:43
  247.0 7.2 %all-gather.5.cloned.1.call-done = bf16[512,1024]{1,0:T(8,128)(2,1)} async-done(((bf16[128,1024]{1,0:T(8,128)(2,1)}), bf16[512,1024]{1,0:T(8,128)(2,1)}) %all-gather.5.cloned.1.call-update) | async-done | bytes 1048592 | tf_op jit(solution)/shard_map/all_gather | solution.py:138
  254.2 4.1 %fusion.66 = bf16[512,1024]{1,0:T(8,128)(2,1)} fusion(bf16[512,1024]{1,0:T(8,128)(2,1)} %all-gather.5.cloned.1.call-done, bf16[2,1024,1024]{2,1,0:T(8,128)(2,1)} %param.24), kind=kOutput, calls=%fused_computation.61 | convolution fusion | flops 1074266112 | bytes 4194304 | tf_op jit(solution)/shard_map/dot_general | solution.py:137
  258.4 7.7 %fusion.3 = f32[1,16,4,128,256]{4,3,2,1,0:T(8,128)S(1)} fusion(f32[2,16,4,128,256]{4,3,2,1,0:T(8,128)} %param.25, f32[16,4,128]{2,1,0:T(4,128)S(1)} %exp.57, bf16[16,8,4,256]{3,1,2,0:T(8,128)(2,1)S(1)} %bitcast.211, f32[16,8,4,128]{3,1,2,0:T(8,128)S(1)} %reduce_window_sum.18, bf16[128,512]{1,0:T(8,128)(2,1)S(1)} %get-tuple-element.4, ...), kind=kOutput, calls=%fused_computation.5 | convolution fusion | flops 205783040 | bytes 17498624 | tf_op jit(solution)/shard_map/sjhd,sjhv->shdv/dot_general | solution.py:43
  266.1 9.9 %pad_maximum_fusion = f32[2,16,4,128,256]{4,3,2,1,0:T(8,128)} fusion(f32[1,16,4,128,256]{4,3,2,1,0:T(8,128)S(1)} %fusion.3, f32[1,16,4,128,256]{4,3,2,1,0:T(8,128)} %fusion.7), kind=kLoop, calls=%fused_computation | loop fusion | flops 4194304 | bytes 33554432 | tf_op jit(solution)/shard_map/stack | solution.py:146
  276.0 34.4 %all-reduce.5.cloned.1.call-done = bf16[512,1024]{1,0:T(8,128)(2,1)} async-done(((bf16[512,1024]{1,0:T(8,128)(2,1)}), bf16[512,1024]{1,0:T(8,128)(2,1)}) %all-reduce.5.cloned.1.call-update) | async-done | bytes 1048592 | tf_op jit(solution)/shard_map/psum | solution.py:142
  310.4 2.8 fusion.86
  (94 shorter events, 30.2 us)
Async XLA Ops:
  7.2 67.1 %reduce-scatter.3.cloned.1.call-start = ((), (), s32[]{:S(2)}) async-start(), calls=%async_computation.2 | async-start | bytes 4587520 | tf_op jit(solution)/shard_map/reduce_scatter | solution.py:95
  18.1 2.7 copy-start
  24.7 4.0 %copy-start.11 = (bf16[2,1024,1024]{2,1,0:T(8,128)(2,1)S(1)}, bf16[2,1024,1024]{2,1,0:T(8,128)(2,1)}, u32[]{:S(2)}) copy-start(bf16[2,1024,1024]{2,1,0:T(8,128)(2,1)} %param.19) | copy-start | bytes 12582916
  28.7 2.3 copy-start.15
  32.6 0.7 copy-start.9
  32.6 0.8 copy-start.5
  32.6 0.9 copy-start.8
  32.6 1.5 copy-start.7
  32.6 72.4 %all-gather.3.cloned.1.call-start = ((), (), s32[]{:S(2)}) async-start(), calls=%async_computation.3 | async-start | bytes 1310720 | tf_op jit(solution)/shard_map/all_gather | solution.py:138
  88.2 73.1 %all-reduce.3.cloned.1.call-start = ((), (), s32[]{:S(2)}) async-start(), calls=%async_computation.4 | async-start | bytes 2097152 | tf_op jit(solution)/shard_map/psum | solution.py:142
  109.2 111.0 %reduce-scatter.5.cloned.1.call-start = ((), (), s32[]{:S(2)}) async-start(), calls=%async_computation.5 | async-start | bytes 4587520 | tf_op jit(solution)/shard_map/reduce_scatter | solution.py:95
  161.2 8.6 %copy-start.1 = (bf16[512,1024]{1,0:T(8,128)(2,1)S(1)}, bf16[512,1024]{1,0:T(8,128)(2,1)}, u32[]{:S(2)}) copy-start(bf16[512,1024]{1,0:T(8,128)(2,1)} %all-reduce.3.cloned.1.call-done) | copy-start | bytes 3145732
  169.8 1.6 copy-start.13
  169.8 3.1 copy-start.14
  171.4 3.0 copy-start.10
  174.4 2.2 copy-start.12
  176.7 2.2 copy-start.16
  180.4 73.8 %all-gather.5.cloned.1.call-start = ((), (), s32[]{:S(2)}) async-start(), calls=%async_computation.6 | async-start | bytes 1310720 | tf_op jit(solution)/shard_map/all_gather | solution.py:138
  226.7 1.0 copy-start.3
  226.7 1.0 copy-start.4
  229.6 6.7 %copy-start.6 = (f32[1,256]{1,0:T(1,128)S(1)}, f32[1,256]{1,0:T(1,128)}, u32[]{:S(2)}) copy-start(f32[1,256]{1,0:T(1,128)} %get-tuple-element.18) | copy-start | bytes 3076
  229.6 6.8 %copy-start.2 = (bf16[128,1024]{1,0:T(8,128)(2,1)S(1)}, bf16[128,1024]{1,0:T(8,128)(2,1)}, u32[]{:S(2)}) copy-start(bf16[128,1024]{1,0:T(8,128)(2,1)} %get-tuple-element.2) | copy-start | bytes 786436
  237.3 73.1 %all-reduce.5.cloned.1.call-start = ((), (), s32[]{:S(2)}) async-start(), calls=%async_computation.7 | async-start | bytes 2097152 | tf_op jit(solution)/shard_map/psum | solution.py:142
Sparse Core Ops, SparseCore 0:
  32.7 41.5 reduce-scatter.2
  88.3 16.6 all-gather.2
  109.3 51.8 all-reduce.2
  180.5 39.5 reduce-scatter.4
  237.5 16.6 all-gather.4
  258.5 51.8 all-reduce.4
where the time goes:
time: 321 us; the launch traced here: 320 us
  waiting for transfers between devices  190 us (59%)
  matrix products  60.7 us (19%)
  other arithmetic  29.4 us (9%)
  blocking collectives  15.2 us (5%)
  between operations  14.4 us (4%)
  local copies, waits for them, and re-layouts  9.44 us (3%)
    psum x2, waiting for transfers between devices, shards(): lax.psum(partial_value.astype(jnp.bfloat16), 'tp').astype(jnp.float32)  86.5 us
    reduce_scatter x2, waiting for transfers between devices, shards(): lax.psum_scatter(jnp.concatenate([jnp.dot(normed, matrix, preferred_eleme...  79.9 us
    all_gather x2, waiting for transfers between devices, shards(): lax.all_gather(gated_rows, 'dp', axis=0, tiled=True)  23.8 us
    dot_general x10, matrix products, shards(): jnp.dot(normed, matrix, preferred_element_type=jnp.float32)  21.4 us
    dot_general x2, matrix products, advance(): jnp.einsum('sjhd,sjhv->shdv', weighted, value_rows, precision=lax.Precisi...  17 us
    psum x2, blocking collectives, shards(): square_sum = lax.psum(jnp.sum(stream_f * stream_f, axis=1), 'dp')  15.2 us
    dot_general x2, matrix products, advance(): jnp.einsum('sihd,shdv->sihv', query_rows * jnp.exp(cumulative), carried,...  13.2 us
    another operation x1, other arithmetic, shards(): jnp.stack(new_states, axis=0)  9.87 us
  transfers between devices with their start and end apart: 6, of which 6 were waited for; matrix products, arithmetic and copies ran while one was open for 9% of the time, Pallas kernels for 0%

commit v1 on v0

v1 whole, which is shorter than its diff:
```python
import functools
import jax
import jax.numpy as jnp
from jax import lax
from jax.experimental import pallas as pl
from jax.experimental.pallas import tpu as pltpu
from jax.sharding import PartitionSpec as P

LAYERS = 2
EPS = 1e-06
TAU = 16.0
MESH = pl.DeviceIdType.MESH
F32 = jnp.float32
BF16 = jnp.bfloat16


def flip(me, bits):
    out, bit = me, 1
    while bit <= bits:
        if bits & bit:
            out = out + bit * (1 - 2 * (lax.div(me, bit) % 2))
        bit *= 2
    return out


def slots_of(n):
    table = {}
    for k in range(n.bit_length() - 1):
        for t in range(n >> (k + 1)):
            table[k, t] = len(table)
    return table


def greet(n, axis, me):
    barrier = pltpu.get_barrier_semaphore()
    steps = n.bit_length() - 1
    for k in range(steps):
        pl.semaphore_signal(barrier, inc=1, device_id={axis: flip(me, 1 << k)}, device_id_type=MESH)
    pl.semaphore_wait(barrier, steps)


def scatter_kernel(n, axis, x_ref, ss_ref, y_ref, sso_ref, rbuf, rss, sbuf, sss, send, recv, ssend, srecv):
    me = lax.axis_index(axis)
    slots = slots_of(n)
    steps = n.bit_length() - 1
    rows = x_ref.shape[1]
    piece = 16 if rows % 16 == 0 else rows
    greet(n, axis, me)
    copies = {}
    waited = set()

    def arrive(key):
        if key not in waited:
            waited.add(key)
            for c in copies[key]:
                c.wait_recv()

    for k in range(steps):
        peer = flip(me, 1 << k)
        for t in reversed(range(n >> (k + 1))):
            slot = slots[k, t]
            bits = (1 << k) | (t << (k + 1))
            chunk = flip(me, bits)
            if k == 0:
                src, ssrc = x_ref.at[chunk], ss_ref.at[chunk]
            else:
                terms = [(j, bits >> (j + 1)) for j in range(k)]
                for term in terms:
                    arrive(term)
                places = [slots[term] for term in terms]
                out = slot - slots[1, 0]

                @pl.loop(0, rows // piece)
                def _(i):
                    at = pl.ds(pl.multiple_of(i * piece, piece), piece)
                    total = x_ref[chunk, at, :].astype(F32)
                    for place in places:
                        total += rbuf[place, at, :].astype(F32)
                    sbuf[out, at, :] = total.astype(BF16)

                small = ss_ref[chunk]
                for place in places:
                    small += rss[place]
                sss[out] = small
                src, ssrc = sbuf.at[out], sss.at[out]
            pair = [
                pltpu.make_async_remote_copy(ssrc, rss.at[slot], ssend.at[slot], srecv.at[slot],
                                             device_id={axis: peer}, device_id_type=MESH),
                pltpu.make_async_remote_copy(src, rbuf.at[slot], send.at[slot], recv.at[slot],
                                             device_id={axis: peer}, device_id_type=MESH),
            ]
            for c in pair:
                c.start()
            copies[k, t] = pair
    places = [slots[k, 0] for k in range(steps)]
    for key in slots:
        arrive(key)

    @pl.loop(0, rows // piece)
    def _(i):
        at = pl.ds(pl.multiple_of(i * piece, piece), piece)
        total = x_ref[me, at, :].astype(F32)
        for place in places:
            total += rbuf[place, at, :].astype(F32)
        y_ref[at, :] = total.astype(BF16)

    small = ss_ref[me]
    for place in places:
        small += rss[place]
    sso_ref[...] = small
    for pair in copies.values():
        for c in pair:
            c.wait_send()


def reduce_scatter(n, axis, x, ss, cid):
    _, m, cols = x.shape
    count = len(slots_of(n))
    held = max(1, count - n // 2)
    vm = pl.BlockSpec(memory_space=pltpu.VMEM)
    dma = pltpu.SemaphoreType.DMA((count,))
    return pl.pallas_call(
        functools.partial(scatter_kernel, n, axis),
        out_shape=(jax.ShapeDtypeStruct((m, cols), BF16), jax.ShapeDtypeStruct((1, m), F32)),
        in_specs=[vm, vm],
        out_specs=(vm, vm),
        scratch_shapes=[
            pltpu.VMEM((count, m, cols), BF16), pltpu.VMEM((count, 1, m), F32),
            pltpu.VMEM((held, m, cols), BF16), pltpu.VMEM((held, 1, m), F32),
            dma, dma, dma, dma,
        ],
        compiler_params=pltpu.CompilerParams(collective_id=cid, has_side_effects=True),
    )(x, ss)


def gather_kernel(n, axis, g_ref, live_ref, o_ref, lo_ref, buf, lbuf, send, recv, lsend, lrecv):
    me = lax.axis_index(axis)
    slots = slots_of(n)
    steps = n.bit_length() - 1
    greet(n, axis, me)
    copies = {}

    def push(k, bits):
        t = bits >> (k + 1)
        slot = slots[k, t]
        chunk = flip(me, bits)
        src = g_ref if bits == 0 else buf.at[chunk]
        lsrc = live_ref if bits == 0 else lbuf.at[chunk]
        peer = {axis: flip(me, 1 << k)}
        pair = [
            pltpu.make_async_remote_copy(lsrc, lbuf.at[chunk], lsend.at[slot], lrecv.at[slot],
                                         device_id=peer, device_id_type=MESH),
            pltpu.make_async_remote_copy(src, buf.at[chunk], send.at[slot], recv.at[slot],
                                         device_id=peer, device_id_type=MESH),
        ]
        for c in pair:
            c.start()
        copies[k, t] = pair

    for k in reversed(range(steps)):
        push(k, 0)
    o_ref[me] = g_ref[...]
    lo_ref[me] = live_ref[...]
    for k in reversed(range(steps)):
        for t in range(n >> (k + 1)):
            for c in copies[k, t]:
                c.wait_recv()
            bits = (1 << k) | (t << (k + 1))
            for j in reversed(range(k)):
                push(j, bits)
            chunk = flip(me, bits)
            o_ref[chunk] = buf[chunk]
            lo_ref[chunk] = lbuf[chunk]
    for pair in copies.values():
        for c in pair:
            c.wait_send()


def all_gather(n, axis, g, live, cid):
    m, cols = g.shape
    count = len(slots_of(n))
    vm = pl.BlockSpec(memory_space=pltpu.VMEM)
    dma = pltpu.SemaphoreType.DMA((count,))
    return pl.pallas_call(
        functools.partial(gather_kernel, n, axis),
        out_shape=(jax.ShapeDtypeStruct((n, m, cols), BF16), jax.ShapeDtypeStruct((n, 1, m), F32)),
        in_specs=[vm, vm],
        out_specs=(vm, vm),
        scratch_shapes=[pltpu.VMEM((n, m, cols), BF16), pltpu.VMEM((n, 1, m), F32), dma, dma, dma, dma],
        compiler_params=pltpu.CompilerParams(collective_id=cid, has_side_effects=True),
    )(g, live)


def shift_rows(x, d):
    return x if d == 0 else pltpu.roll(x, d, 0)


def recurrence_kernel(heads, dk, dv, new, y_ref, scale_ref, live_ref, bias_ref, extra_ref, gain_ref, s_ref, *rest):
    g_ref, out_ref = rest[-2:]
    rows = y_ref.shape[0]
    seqs = rows // new
    kc, vc = heads * dk, heads * dv
    scale = scale_ref[...]
    live = live_ref[...]
    slot = lax.broadcasted_iota(jnp.int32, (rows, 1), 0) % new
    rowid = lax.broadcasted_iota(jnp.int32, (rows, 1), 0) // new
    for h in range(heads):
        ks, vs = pl.ds(h * dk, dk), h * dv
        q = y_ref[:, h * dk:(h + 1) * dk].astype(F32) * (scale * dk ** -0.5)
        k = y_ref[:, kc + h * dk:kc + (h + 1) * dk].astype(F32) * (scale * live)
        v = y_ref[:, 2 * kc + vs:2 * kc + vs + dv].astype(F32) * scale
        r = y_ref[:, 2 * kc + vc + vs:2 * kc + vc + vs + dv].astype(F32) * scale
        logit = y_ref[:, 2 * kc + 2 * vc + h * dk:2 * kc + 2 * vc + (h + 1) * dk].astype(F32) * scale
        z = logit + bias_ref[0, :, ks]
        logsig = jnp.minimum(z, 0.0) - jnp.log1p(jnp.exp(-jnp.abs(z)))
        a = (logsig / TAU + extra_ref[:, h:h + 1]) * live
        c, d = a, 1
        while d < new:
            c = c + jnp.where(slot >= d, shift_rows(c, d), 0.0)
            d *= 2
        last = c.reshape(seqs, new, dk)[:, new - 1:new, :]
        last = jnp.broadcast_to(last, (seqs, new, dk)).reshape(rows, dk)
        o = jnp.zeros((rows, dv), F32)
        for d in range(new):
            ok = slot >= d
            gap = jnp.where(ok, c - shift_rows(c, d), 0.0)
            s = jnp.sum(q * shift_rows(k, d) * jnp.exp(gap), axis=1, keepdims=True)
            o = o + jnp.where(ok, s, 0.0) * shift_rows(v, d)
        qe = (q * jnp.exp(c)).astype(BF16)
        ke = (k * jnp.exp(last - c)).T.astype(BF16)
        el = jnp.exp(last).T
        parts = []
        for i in range(seqs):
            state = s_ref[0, i, h]
            parts.append(jnp.dot(qe[i * new:(i + 1) * new], state.astype(BF16), preferred_element_type=F32))
            vm = jnp.where(rowid == i, v, 0.0).astype(BF16)
            upd = jnp.dot(ke, vm, preferred_element_type=F32)
            out_ref[0, i, h] = el[:, i * new:i * new + 1] * state + upd
        o = o + jnp.concatenate(parts, axis=0)
        norm = o * lax.rsqrt(jnp.mean(o * o, axis=1, keepdims=True) + EPS) * gain_ref[0].astype(F32)
        g_ref[:, vs:vs + dv] = (norm * (r * jax.nn.sigmoid(r)) * live).astype(BF16)


def recurrence(layer, y, scale, live, bias, extra, gains, grid, states):
    layers, seqs, heads, dk, dv = grid.shape
    new = y.shape[0] // seqs
    block = 4 if seqs % 4 == 0 else 1
    rows = block * new
    cols = y.shape[1]
    by_row = lambda width: pl.BlockSpec((rows, width), lambda b: (b, 0))
    state_spec = pl.BlockSpec((1, block, heads, dk, dv), lambda b: (layer, b, 0, 0, 0))
    args = [y, scale, live, bias.reshape(layers, 1, -1), extra, gains.reshape(layers, 1, -1), grid]
    in_specs = [
        by_row(cols), by_row(1), by_row(1),
        pl.BlockSpec((1, 1, heads * dk), lambda b: (layer, 0, 0)),
        by_row(heads),
        pl.BlockSpec((1, 1, dv), lambda b: (layer, 0, 0)),
        state_spec,
    ]
    alias = {}
    if states is not None:
        args.append(states)
        in_specs.append(pl.BlockSpec(memory_space=pl.ANY))
        alias = {len(args) - 1: 1}
    return pl.pallas_call(
        functools.partial(recurrence_kernel, heads, dk, dv, new),
        grid=(seqs // block,),
        out_shape=(jax.ShapeDtypeStruct((seqs * new, heads * dv), BF16), jax.ShapeDtypeStruct(grid.shape, F32)),
        in_specs=in_specs,
        out_specs=(by_row(heads * dv), state_spec),
        input_output_aliases=alias,
        compiler_params=pltpu.CompilerParams(dimension_semantics=("arbitrary",)),
    )(*args)


def shards(x0, lengths, norm_gains, wq, wk, wv, wr, wa, bias, extra, head_gains, wo, grid):
    streams, new, width = x0.shape
    lines = streams * new
    seqs = lengths.shape[0]
    rows = seqs * new
    n = lines // rows
    full = width * n
    x = x0.reshape(lines, width)
    live = (lax.broadcasted_iota(jnp.int32, (seqs, new), 1) < lengths[:, None]).astype(F32)
    live_col, live_row = live.reshape(rows, 1), live.reshape(1, rows)
    extra = extra.reshape(rows, -1)
    states = None
    for l in range(LAYERS):
        xf = x.astype(F32)
        ss = jnp.sum(xf * xf, axis=1).reshape(n, 1, rows)
        scaled = (xf * norm_gains[l].astype(F32)).astype(BF16)
        partial = jnp.concatenate(
            [jnp.dot(scaled, w[l], preferred_element_type=F32).astype(BF16) for w in (wq, wk, wv, wr, wa)], axis=1)
        y, total = reduce_scatter(n, "dp", partial.reshape(n, rows, -1), ss, 2 * l)
        scale = lax.rsqrt(total / full + EPS).reshape(rows, 1)
        g, states = recurrence(l, y, scale, live_col, bias, extra, head_gains, grid, states)
        every, alive = all_gather(n, "dp", g, live_row, 2 * l + 1)
        alive = alive.reshape(1, lines)
        rank = jnp.cumsum(alive, axis=1) - 1.0
        index = lax.broadcasted_iota(jnp.int32, (lines // 2, lines), 0).astype(F32)
        pick = ((rank == index) & (alive > 0)).astype(BF16)
        packed = jnp.dot(pick, every.reshape(lines, -1), preferred_element_type=F32).astype(BF16)
        mixed = lax.psum(jnp.dot(packed, wo[l], preferred_element_type=F32).astype(BF16), "tp")
        spread = lax.dot_general(pick, mixed, (((0,), (0,)), ((), ())), preferred_element_type=F32)
        x = (xf + spread).astype(BF16)
    return x.reshape(streams, new, width), states


def solution(mesh):
    in_specs = (
        P("grp", None, "dp"),
        P(("grp", "dp")),
        P(None, "dp"),
        P(None, "dp", "tp"),
        P(None, "dp", "tp"),
        P(None, "dp", "tp"),
        P(None, "dp", "tp"),
        P(None, "dp", "tp"),
        P(None, "tp"),
        P(("grp", "dp"), None, "tp"),
        P(),
        P(None, "tp", "dp"),
        P(None, ("grp", "dp"), "tp", None, None),
    )
    out_specs = (P("grp", None, "dp"), P(None, ("grp", "dp"), "tp", None, None))
    return jax.shard_map(shards, mesh=mesh, in_specs=in_specs, out_specs=out_specs, check_vma=False)
```

time: 321 us -> 250 us (0.78)
  waiting for transfers between devices: 190 us -> 77.6 us
  Pallas kernels: 0 us -> 102 us
  matrix products: 60.7 us -> 35.2 us
  other arithmetic: 29.4 us -> 7.96 us
  blocking collectives: 15.2 us -> 0 us
    pallas_call x0 -> x6, Pallas kernels: none -> 102 us  [the longest x2 58.4 us: reduce_scatter(): pl.pallas_call(functools.partial(scatter_kernel, n, axis), out_shape=(jax...]
    reduce_scatter x2 -> x0, waiting for transfers between devices: 79.9 us -> none  [shards(): lax.psum_scatter(jnp.concatenate([jnp.dot(normed, matrix, preferred_eleme...]
    dot_general x18 -> x14, matrix products: 60.7 us -> 35.2 us  [the longest x10 22.9 us: shards(): jnp.dot(scaled, w[l], preferred_element_type=F32).astype(BF16)]
    all_gather x2 -> x0, waiting for transfers between devices: 23.8 us -> none  [shards(): lax.all_gather(gated_rows, 'dp', axis=0, tiled=True)]
    psum x2 -> x0, blocking collectives: 15.2 us -> none  [shards(): square_sum = lax.psum(jnp.sum(stream_f * stream_f, axis=1), 'dp')]
    another operation x3 -> x4, other arithmetic: 11.3 us -> 2.31 us  [the longest x1 9.87 us: shards(): jnp.stack(new_states, axis=0)]
    psum x2, waiting for transfers between devices: 86.5 us -> 77.6 us  [shards(): lax.psum(jnp.dot(packed, wo[l], preferred_element_type=F32).astype(BF16),...]
    slice x7 -> x1, local copies, waits for them, and re-layouts: 4.87 us -> 0.19 us  [the longest x2 2.83 us: shards(): summed[:, 2 * key_cols + value_cols:2 * key_cols + 2 * value_cols]]
  transfers between devices with their start and end apart: 6 -> 2, of which waited for: 6 -> 2; matrix products, arithmetic and copies ran while one was open for 9% -> 0% of each run, Pallas kernels for 0% -> 0%
where the time goes in v1:
time: 250 us; the launch traced here: 249 us
  Pallas kernels  102 us (41%)
  waiting for transfers between devices  77.6 us (31%)
  matrix products  35.2 us (14%)
  between operations  14.2 us (6%)
  local copies, waits for them, and re-layouts  12.3 us (5%)
  other arithmetic  7.96 us (3%)
    psum x2, waiting for transfers between devices, shards(): lax.psum(jnp.dot(packed, wo[l], preferred_element_type=F32).astype(BF16),...  77.6 us
    pallas_call x2, Pallas kernels, reduce_scatter(): pl.pallas_call(functools.partial(scatter_kernel, n, axis), out_shape=(jax...  58.4 us
    pallas_call x2, Pallas kernels, all_gather(): pl.pallas_call(functools.partial(gather_kernel, n, axis), out_shape=(jax....  23.1 us
    dot_general x10, matrix products, shards(): jnp.dot(scaled, w[l], preferred_element_type=F32).astype(BF16)  22.9 us
    pallas_call x2, Pallas kernels, recurrence(): pl.pallas_call(functools.partial(recurrence_kernel, heads, dk, dv, new),...  20.3 us
    dot_general x2, matrix products, shards(): jnp.dot(packed, wo[l], preferred_element_type=F32).astype(BF16)  7.49 us
  transfers between devices with their start and end apart: 2, of which 2 were waited for; matrix products, arithmetic and copies ran while one was open for 0% of the time, Pallas kernels for 0%

profile of v1, /device:TPU:0, one launch (start us, length us, event | category | flops | bytes accessed | tf_op | source)
XLA Modules:
  0.0 249.4 jit_solution(9791002983948724446)
XLA Ops:
  10.6 1.3 reshape.230.bias_ref
  12.6 1.5 fusion.6
  14.8 1.4 copy.31
  16.2 2.4 convolution_convert_fusion.6
  18.9 2.0 convolution_convert_fusion.7
  22.7 4.0 %fusion.28 = bf16[512,3584]{1,0:T(8,128)(2,1)} fusion(bf16[512,3584]{1,0:T(8,128)(2,1)} %constant_dynamic-update-slice_fusion, bf16[2,1024,1024]{2,1,0:T(8,128)(2,1)} %param.18, bf16[64,8,1024]{2,1,0:T(8,128)(2,1)S(1)} %copy-done, f32[1024]{0:T(1024)S(1)} %bitcast.123), kind=kOutput, calls=%fused_computation.32 | convolution fusion | flops 1075838976 | bytes 4198400 | tf_op jit(solution)/shard_map/dot_general | solution.py:293
  26.7 2.3 fusion.34
  29.0 1.5 fusion.57
  30.5 29.7 %shard_map.140 = (bf16[128,3584]{1,0:T(8,128)(2,1)}, f32[1,128]{1,0:T(1,128)}) custom-call(bf16[4,128,3584]{2,1,0:T(8,128)(2,1)} %bitcast.8.x_ref, f32[4,1,128]{2,1,0:T(1,128)} %bitcast.111), custom_call_target="tpu_custom_call" | custom-call | tf_op jit(solution)/shard_map/pallas_call | solution.py:122
  61.6 10.2 %shard_map.141 = (bf16[128,1024]{1,0:T(8,128)(2,1)}, f32[2,16,4,128,256]{4,3,2,1,0:T(8,128)}) custom-call(bf16[128,3584]{1,0:T(8,128)(2,1)} %get-tuple-element.14.y_ref, f32[128,1]{1,0:T(8,128)} %copy.32.scale_ref, f32[128,1]{1,0:T(8,128)} %reshape.254.live_ref, f32[2,1,512]{2,1,0:T(1,128)} %reshape.230.bias_ref, f32[128,4]{1,0:T(8,128)} %bitcast.109, ...), custom_call_target="tpu_custom_call" | custom-call | tf_op jit(solution)/shard_map/pallas_call | solution.py:265
  71.7 11.7 %shard_map.142 = (bf16[4,128,1024]{2,1,0:T(8,128)(2,1)}, f32[4,1,128]{2,1,0:T(1,128)}) custom-call(bf16[128,1024]{1,0:T(8,128)(2,1)} %get-tuple-element.16.g_ref, f32[1,128]{1,0:T(1,128)} %reshape.252.live_ref), custom_call_target="tpu_custom_call" | custom-call | tf_op jit(solution)/shard_map/pallas_call | solution.py:184
  85.5 3.7 %fusion.50 = bf16[256,1024]{1,0:T(8,128)(2,1)} fusion(bf16[2,1024,1024]{2,1,0:T(8,128)(2,1)} %param.24, bf16[512,1024]{1,0:T(8,128)(2,1)} %bitcast.135, f32[512]{0:T(512)S(1)} %fusion.101, f32[256]{0:T(256)S(1)} %iota_convert_fusion, pred[512]{0:T(512)(128)(4,1)S(1)} %bitcast.130), kind=kOutput, calls=%fused_computation.42 | convolution fusion | flops 806092800 | bytes 3673600 | tf_op jit(solution)/shard_map/dot_general | solution.py:303
  89.5 39.6 %all-reduce.3.cloned.1.call-done = bf16[256,1024]{1,0:T(8,128)(2,1)} async-done(((bf16[256,1024]{1,0:T(8,128)(2,1)}), bf16[256,1024]{1,0:T(8,128)(2,1)}) %all-reduce.3.cloned.1.call-update) | async-done | bytes 524304 | tf_op jit(solution)/shard_map/psum | solution.py:303
  129.1 2.3 fusion.1
  131.4 2.1 convolution_convert_fusion.3
  136.5 4.0 %fusion.40 = bf16[512,3584]{1,0:T(8,128)(2,1)} fusion(bf16[512,3584]{1,0:T(8,128)(2,1)} %constant_dynamic-update-slice_fusion.2, bf16[2,1024,1024]{2,1,0:T(8,128)(2,1)} %param.18, bf16[512,1024]{1,0:T(8,128)(2,1)S(1)} %get-tuple-element.29, f32[1024]{0:T(1024)S(1)} %bitcast.118), kind=kOutput, calls=%fused_computation.36 | convolution fusion | flops 1075838976 | bytes 4198400 | tf_op jit(solution)/shard_map/dot_general | solution.py:293
  140.5 2.3 fusion.46
  142.8 1.5 fusion.56
  144.4 28.7 %shard_map.143 = (bf16[128,3584]{1,0:T(8,128)(2,1)}, f32[1,128]{1,0:T(1,128)}) custom-call(bf16[4,128,3584]{2,1,0:T(8,128)(2,1)} %bitcast.25.x_ref, f32[4,1,128]{2,1,0:T(1,128)} %bitcast.126), custom_call_target="tpu_custom_call" | custom-call | tf_op jit(solution)/shard_map/pallas_call | solution.py:122
  174.4 10.2 %shard_map.144 = (bf16[128,1024]{1,0:T(8,128)(2,1)}, f32[2,16,4,128,256]{4,3,2,1,0:T(8,128)}) custom-call(bf16[128,3584]{1,0:T(8,128)(2,1)} %get-tuple-element.19.y_ref, f32[128,1]{1,0:T(8,128)} %copy.38.scale_ref, f32[128,1]{1,0:T(8,128)} %reshape.254.live_ref, f32[2,1,512]{2,1,0:T(1,128)} %reshape.230.bias_ref, ...), custom_call_target="tpu_custom_call", output_to_operand_aliasing={{1}: (7, {})} | custom-call | tf_op jit(solution)/shard_map/pallas_call | solution.py:265
  184.6 11.4 %shard_map.145 = (bf16[4,128,1024]{2,1,0:T(8,128)(2,1)}, f32[4,1,128]{2,1,0:T(1,128)}) custom-call(bf16[128,1024]{1,0:T(8,128)(2,1)} %get-tuple-element.22.g_ref, f32[1,128]{1,0:T(1,128)} %reshape.252.live_ref), custom_call_target="tpu_custom_call" | custom-call | tf_op jit(solution)/shard_map/pallas_call | solution.py:184
  198.2 3.7 %fusion.53 = bf16[256,1024]{1,0:T(8,128)(2,1)} fusion(bf16[2,1024,1024]{2,1,0:T(8,128)(2,1)} %param.24, bf16[512,1024]{1,0:T(8,128)(2,1)} %bitcast.134, f32[512]{0:T(512)S(1)} %fusion.100, f32[256]{0:T(256)S(1)} %iota_convert_fusion, pred[512]{0:T(512)(128)(4,1)S(1)} %bitcast.127), kind=kOutput, calls=%fused_computation.43 | convolution fusion | flops 806092800 | bytes 3673600 | tf_op jit(solution)/shard_map/dot_general | solution.py:303
  201.9 38.0 %all-reduce.5.cloned.1.call-done = bf16[256,1024]{1,0:T(8,128)(2,1)} async-done(((bf16[256,1024]{1,0:T(8,128)(2,1)}), bf16[256,1024]{1,0:T(8,128)(2,1)}) %all-reduce.5.cloned.1.call-update) | async-done | bytes 524304 | tf_op jit(solution)/shard_map/psum | solution.py:303
  240.0 2.6 %fusion.49 = bf16[64,8,1024]{2,1,0:T(8,128)(2,1)} fusion(bf16[256,1024]{1,0:T(8,128)(2,1)} %all-reduce.5.cloned.1.call-done, bf16[512,1024]{1,0:T(8,128)(2,1)S(1)} %get-tuple-element.29, f32[512]{0:T(512)S(1)} %fusion.100, f32[256]{0:T(256)S(1)} %iota_convert_fusion, pred[512]{0:T(512)(128)(4,1)S(1)} %bitcast.128), kind=kOutput, calls=%fused_computation.39 | convolution fusion | flops 270270464 | bytes 2625024 | tf_op jit(solution)/shard_map/dot_general | solution.py:304
  (50 shorter events, 17.1 us)
Async XLA Ops:
  7.2 122.0 %all-reduce.3.cloned.1.call-start = ((), (), s32[]{:S(2)}) async-start(), calls=%async_computation | async-start | bytes 1048576 | tf_op jit(solution)/shard_map/psum | solution.py:303
  16.2 2.6 %copy-start = (bf16[64,8,1024]{2,1,0:T(8,128)(2,1)S(1)}, bf16[64,8,1024]{2,1,0:T(8,128)(2,1)}, u32[]{:S(2)}) copy-start(bf16[64,8,1024]{2,1,0:T(8,128)(2,1)} %param.13) | copy-start | bytes 3145732
  22.7 4.0 %copy-start.1 = (bf16[2,1024,1024]{2,1,0:T(8,128)(2,1)S(1)}, bf16[2,1024,1024]{2,1,0:T(8,128)(2,1)}, u32[]{:S(2)}) copy-start(bf16[2,1024,1024]{2,1,0:T(8,128)(2,1)} %param.19) | copy-start | bytes 12582916
  26.7 2.3 copy-start.4
  89.3 150.6 %all-reduce.5.cloned.1.call-start = ((), (), s32[]{:S(2)}) async-start(), calls=%async_computation.1 | async-start | bytes 1048576 | tf_op jit(solution)/shard_map/psum | solution.py:303
  131.4 2.1 copy-start.3
  136.5 4.0 %copy-start.2 = (bf16[2,1024,1024]{2,1,0:T(8,128)(2,1)S(1)}, bf16[2,1024,1024]{2,1,0:T(8,128)(2,1)}, u32[]{:S(2)}) copy-start(bf16[2,1024,1024]{2,1,0:T(8,128)(2,1)} %param.19) | copy-start | bytes 12582916
  140.5 2.3 copy-start.5
Sparse Core Ops, SparseCore 0:
  89.4 39.6 all-reduce.2
  202.0 37.8 all-reduce.4

commit v2 on v1

--- a/solution.py
+++ b/solution.py
@@ -121,16 +121,124 @@
     dma = pltpu.SemaphoreType.DMA((count,))
     return pl.pallas_call(
         functools.partial(scatter_kernel, n, axis),
-        out_shape=(jax.ShapeDtypeStruct((m, cols), BF16), jax.ShapeDtypeStruct((1, m), F32)),
+        out_shape=(jax.ShapeDtypeStruct((m, cols), BF16), jax.ShapeDtypeStruct(ss.shape[1:], F32)),
         in_specs=[vm, vm],
         out_specs=(vm, vm),
         scratch_shapes=[
-            pltpu.VMEM((count, m, cols), BF16), pltpu.VMEM((count, 1, m), F32),
-            pltpu.VMEM((held, m, cols), BF16), pltpu.VMEM((held, 1, m), F32),
+            pltpu.VMEM((count, m, cols), BF16), pltpu.VMEM((count,) + ss.shape[1:], F32),
+            pltpu.VMEM((held, m, cols), BF16), pltpu.VMEM((held,) + ss.shape[1:], F32),
             dma, dma, dma, dma,
         ],
         compiler_params=pltpu.CompilerParams(collective_id=cid, has_side_effects=True),
     )(x, ss)
+
+
+def project_kernel(n, axis, layer, plan, h_ref, ss_ref, *rest):
+    weights = rest[:5]
+    y_ref, sso_ref, wbuf, xbuf, rbuf, rss, sbuf, sss, load, send, recv, ssend, srecv = rest[5:]
+    me = lax.axis_index(axis)
+    slots = slots_of(n)
+    steps = n.bit_length() - 1
+    segs, wide = len(plan), wbuf.shape[2]
+    loads = []
+    for s, (which, start) in enumerate(plan):
+        c = pltpu.make_async_copy(weights[which].at[layer, :, pl.ds(start, wide)], wbuf.at[s], load.at[s])
+        c.start()
+        loads.append(c)
+    greet(n, axis, me)
+    copies = {}
+    waited = set()
+
+    def arrive(key):
+        if key not in waited:
+            waited.add(key)
+            for c in copies[key]:
+                c.wait_recv()
+
+    def step(k, s):
+        peer = {axis: flip(me, 1 << k)}
+        for t in reversed(range(n >> (k + 1))):
+            slot = slots[k, t]
+            bits = (1 << k) | (t << (k + 1))
+            chunk = flip(me, bits)
+            if k == 0:
+                src, ssrc = xbuf.at[s, chunk], ss_ref.at[chunk]
+            else:
+                terms = [(j, bits >> (j + 1)) for j in range(k)]
+                out = slot - slots[1, 0]
+                total = xbuf[s, chunk].astype(F32)
+                for term in terms:
+                    arrive(term + (s,))
+                    total += rbuf[slots[term], s].astype(F32)
+                sbuf[out, s] = total.astype(BF16)
+                src, ssrc = sbuf.at[out, s], sss.at[out]
+                if s == 0:
+                    small = ss_ref[chunk]
+                    for term in terms:
+                        small += rss[slots[term]]
+                    sss[out] = small
+            group = []
+            if s == 0:
+                group.append(pltpu.make_async_remote_copy(
+                    ssrc, rss.at[slot], ssend.at[slot], srecv.at[slot], device_id=peer, device_id_type=MESH))
+            group.append(pltpu.make_async_remote_copy(
+                src, rbuf.at[slot, s], send.at[slot, s], recv.at[slot, s], device_id=peer, device_id_type=MESH))
+            for c in group:
+                c.start()
+            copies[k, t, s] = group
+
+    for turn in range(segs + steps - 1):
+        if turn < segs:
+            loads[turn].wait()
+
+            @pl.loop(0, n)
+            def _(i):
+                xbuf[turn, i] = jnp.dot(h_ref[i], wbuf[turn], preferred_element_type=F32).astype(BF16)
+
+            step(0, turn)
+        for k in range(1, steps):
+            if 0 <= turn - k < segs:
+                step(k, turn - k)
+    for s in range(segs):
+        total = xbuf[s, me].astype(F32)
+        for k in range(steps):
+            arrive((k, 0, s))
+            total += rbuf[slots[k, 0], s].astype(F32)
+        y_ref[:, s * wide:(s + 1) * wide] = total.astype(BF16)
+    small = ss_ref[me]
+    for k in range(steps):
+        small += rss[slots[k, 0]]
+    sso_ref[...] = small
+    for key, group in copies.items():
+        arrive(key)
+        for c in group:
+            c.wait_send()
+
+
+def project_scatter(n, axis, layer, h, ss, weights, cid):
+    _, m, depth = h.shape
+    wide = min(w.shape[2] for w in weights)
+    plan = [(i, c) for i, w in enumerate(weights) for c in range(0, w.shape[2], wide)]
+    segs = len(plan)
+    count = len(slots_of(n))
+    held = max(1, count - n // 2)
+    vm = pl.BlockSpec(memory_space=pltpu.VMEM)
+    dma = lambda *shape: pltpu.SemaphoreType.DMA(shape)
+    return pl.pallas_call(
+        functools.partial(project_kernel, n, axis, layer, plan),
+        out_shape=(jax.ShapeDtypeStruct((m, segs * wide), BF16), jax.ShapeDtypeStruct((1, m), F32)),
+        in_specs=[vm, vm] + [pl.BlockSpec(memory_space=pl.ANY)] * 5,
+        out_specs=(vm, vm),
+        scratch_shapes=[
+            pltpu.VMEM((segs, depth, wide), BF16),
+            pltpu.VMEM((segs, n, m, wide), BF16),
+            pltpu.VMEM((count, segs, m, wide), BF16), pltpu.VMEM((count, 1, m), F32),
+            pltpu.VMEM((held, segs, m, wide), BF16), pltpu.VMEM((held, 1, m), F32),
+            dma(segs), dma(count, segs), dma(count, segs), dma(count), dma(count),
+        ],
+        compiler_params=pltpu.CompilerParams(
+            collective_id=cid, has_side_effects=True, vmem_limit_bytes=40 * 1024 * 1024),
+    )(h, ss, *weights)
 
 
 def gather_kernel(n, axis, g_ref, live_ref, o_ref, lo_ref, buf, lbuf, send, recv, lsend, lrecv):
@@ -183,10 +291,10 @@
     dma = pltpu.SemaphoreType.DMA((count,))
     return pl.pallas_call(
         functools.partial(gather_kernel, n, axis),
-        out_shape=(jax.ShapeDtypeStruct((n, m, cols), BF16), jax.ShapeDtypeStruct((n, 1, m), F32)),
+        out_shape=(jax.ShapeDtypeStruct((n, m, cols), BF16), jax.ShapeDtypeStruct((n,) + live.shape, F32)),
         in_specs=[vm, vm],
         out_specs=(vm, vm),
-        scratch_shapes=[pltpu.VMEM((n, m, cols), BF16), pltpu.VMEM((n, 1, m), F32), dma, dma, dma, dma],
+        scratch_shapes=[pltpu.VMEM((n, m, cols), BF16), pltpu.VMEM((n,) + live.shape, F32), dma, dma, dma, dma],
         compiler_params=pltpu.CompilerParams(collective_id=cid, has_side_effects=True),
     )(g, live)
 
@@ -289,18 +397,21 @@
         xf = x.astype(F32)
         ss = jnp.sum(xf * xf, axis=1).reshape(n, 1, rows)
         scaled = (xf * norm_gains[l].astype(F32)).astype(BF16)
-        partial = jnp.concatenate(
-            [jnp.dot(scaled, w[l], preferred_element_type=F32).astype(BF16) for w in (wq, wk, wv, wr, wa)], axis=1)
-        y, total = reduce_scatter(n, "dp", partial.reshape(n, rows, -1), ss, 2 * l)
+        y, total = project_scatter(n, "dp", l, scaled.reshape(n, rows, width), ss, (wq, wk, wv, wr, wa), 4 * l)
         scale = lax.rsqrt(total / full + EPS).reshape(rows, 1)
         g, states = recurrence(l, y, scale, live_col, bias, extra, head_gains, grid, states)
-        every, alive = all_gather(n, "dp", g, live_row, 2 * l + 1)
+        every, alive = all_gather(n, "dp", g, live_row, 4 * l + 1)
         alive = alive.reshape(1, lines)
         rank = jnp.cumsum(alive, axis=1) - 1.0
         index = lax.broadcasted_iota(jnp.int32, (lines // 2, lines), 0).astype(F32)
         pick = ((rank == index) & (alive > 0)).astype(BF16)
         packed = jnp.dot(pick, every.reshape(lines, -1), preferred_element_type=F32).astype(BF16)
-        mixed = lax.psum(jnp.dot(packed, wo[l], preferred_element_type=F32).astype(BF16), "tp")
+        part = jnp.dot(packed, wo[l], preferred_element_type=F32).astype(BF16)
+        heads_n = lax.axis_size("tp")
+        spare = jnp.zeros((heads_n, 1, 128), F32)
+        mine, word = reduce_scatter(heads_n, "tp", part.reshape(heads_n, -1, width), spare, 4 * l + 2)
+        mixed, _ = all_gather(heads_n, "tp", mine, word, 4 * l + 3)
+        mixed = mixed.reshape(-1, width)
         spread = lax.dot_general(pick, mixed, (((0,), (0,)), ((), ())), preferred_element_type=F32)
         x = (xf + spread).astype(BF16)
     return x.reshape(streams, new, width), states

time: 250 us -> 195 us (0.78)
  waiting for transfers between devices: 77.6 us -> 0 us
  Pallas kernels: 102 us -> 154 us
  matrix products: 35.2 us -> 13.1 us
  between operations: 14.2 us -> 0.79 us
  local copies, waits for them, and re-layouts: 12.3 us -> 18.4 us
    psum x2 -> x0, waiting for transfers between devices: 77.6 us -> none  [shards(): lax.psum(jnp.dot(packed, wo[l], preferred_element_type=F32).astype(BF16),...]
    pallas_call x0 -> x2, Pallas kernels: none -> 53.8 us  [project_scatter(): pl.pallas_call(functools.partial(project_kernel, n, axis, layer, plan), o...]
    pallas_call x2, Pallas kernels: 58.4 us -> 33 us  [reduce_scatter(): pl.pallas_call(functools.partial(scatter_kernel, n, axis), out_shape=(jax...]
    pallas_call x2 -> x4, Pallas kernels: 23.1 us -> 46.6 us  [all_gather(): pl.pallas_call(functools.partial(gather_kernel, n, axis), out_shape=(jax....]
    dot_general x12 -> x2, matrix products: 30.3 us -> 7.67 us  [shards(): part = jnp.dot(packed, wo[l], preferred_element_type=F32).astype(BF16)]
    unnamed x17 -> x23, local copies, waits for them, and re-layouts: 4.86 us -> 11.8 us
  transfers between devices with their start and end apart: 2 -> 0, of which waited for: 2 -> 0; matrix products, arithmetic and copies ran while one was open for 0% -> 0% of each run, Pallas kernels for 0% -> 0%
where the time goes in v2:
time: 195 us
  Pallas kernels  154 us (79%)
  local copies, waits for them, and re-layouts  18.4 us (9%)
  matrix products  13.1 us (7%)
  other arithmetic  8.56 us (4%)
    pallas_call x2, Pallas kernels, project_scatter(): pl.pallas_call(functools.partial(project_kernel, n, axis, layer, plan), o...  53.8 us
    pallas_call x4, Pallas kernels, all_gather(): pl.pallas_call(functools.partial(gather_kernel, n, axis), out_shape=(jax....  46.6 us
    pallas_call x2, Pallas kernels, reduce_scatter(): pl.pallas_call(functools.partial(scatter_kernel, n, axis), out_shape=(jax...  33 us
    pallas_call x2, Pallas kernels, recurrence(): pl.pallas_call(functools.partial(recurrence_kernel, heads, dk, dv, new),...  20.3 us
    unnamed x23, local copies, waits for them, and re-layouts  11.8 us
    dot_general x2, matrix products, shards(): part = jnp.dot(packed, wo[l], preferred_element_type=F32).astype(BF16)  7.67 us
    dot_general x2, matrix products, shards(): lax.dot_general(pick, mixed, (((0,), (0,)), ((), ())), preferred_element_...  5.45 us

profile of v2, /device:TPU:0, one launch (start us, length us, event | category | flops | bytes accessed | tf_op | source)
XLA Modules:
  0.0 194.6 jit_solution(3290793240998659067)
XLA Ops:
  0.6 1.3 copy.25.gain_ref
  1.9 1.3 reshape.217.bias_ref
  5.3 1.5 multiply_reduce_fusion
  7.6 1.5 copy.22
  9.1 1.6 convert_element_type.100
  12.5 1.6 copy-done.3
  14.1 1.6 copy-done.5
  15.7 27.6 %shard_map.140 = (bf16[128,3584]{1,0:T(8,128)(2,1)S(1)}, f32[1,128]{1,0:T(1,128)S(1)}) custom-call(bf16[4,128,1024]{2,1,0:T(8,128)(2,1)S(1)} %fusion.7.h_ref, f32[4,1,128]{2,1,0:T(1,128)S(1)} %bitcast.63, bf16[2,1024,512]{2,1,0:T(8,128)(2,1)S(1)} %copy-done.2, bf16[2,1024,512]{2,1,0:T(8,128)(2,1)S(1)} %copy-done.3, bf16[2,1024,1024]{2,1,0:T(8,128)(2,1)S(1)} %copy-done, ...), custom_call_target="tpu_custom_call" | custom-call | tf_op jit(solution)/shard_map/pallas_call | solution.py:227
  45.0 10.2 %shard_map.141 = (bf16[128,1024]{1,0:T(8,128)(2,1)}, f32[2,16,4,128,256]{4,3,2,1,0:T(8,128)}) custom-call(bf16[128,3584]{1,0:T(8,128)(2,1)} %copy-done.8, f32[128,1]{1,0:T(8,128)} %copy.23.scale_ref, f32[128,1]{1,0:T(8,128)} %reshape.246.live_ref, f32[2,1,512]{2,1,0:T(1,128)} %reshape.217.bias_ref, f32[128,4]{1,0:T(8,128)} %bitcast.66, ...), custom_call_target="tpu_custom_call" | custom-call | tf_op jit(solution)/shard_map/pallas_call | solution.py:373
  55.1 11.8 %shard_map.142 = (bf16[4,128,1024]{2,1,0:T(8,128)(2,1)}, f32[4,1,128]{2,1,0:T(1,128)}) custom-call(bf16[128,1024]{1,0:T(8,128)(2,1)} %get-tuple-element.22.g_ref, f32[1,128]{1,0:T(1,128)} %reshape.244.live_ref), custom_call_target="tpu_custom_call" | custom-call | tf_op jit(solution)/shard_map/pallas_call | solution.py:292
  67.6 1.0 reduce-window.14
  69.1 3.8 %fusion.12 = bf16[256,1024]{1,0:T(8,128)(2,1)} fusion(bf16[2,1024,1024]{2,1,0:T(8,128)(2,1)} %param.24, bf16[512,1024]{1,0:T(8,128)(2,1)} %bitcast.85, f32[512]{0:T(512)S(1)} %fusion.38, f32[256]{0:T(256)S(1)} %iota_convert_fusion, pred[512]{0:T(512)(128)(4,1)S(1)} %bitcast.80), kind=kOutput, calls=%fused_computation.20 | convolution fusion | flops 806092800 | bytes 3673600 | tf_op jit(solution)/shard_map/dot_general | solution.py:409
  73.5 16.4 %shard_map.143 = (bf16[64,1024]{1,0:T(8,128)(2,1)}, f32[1,128]{1,0:T(1,128)}) custom-call(bf16[4,64,1024]{2,1,0:T(8,128)(2,1)} %bitcast.68, f32[4,1,128]{2,1,0:T(1,128)} %broadcast.78.ss_ref), custom_call_target="tpu_custom_call" | custom-call | tf_op jit(solution)/shard_map/pallas_call | solution.py:122
  89.9 12.1 %shard_map.144 = (bf16[4,64,1024]{2,1,0:T(8,128)(2,1)}, f32[4,1,128]{2,1,0:T(1,128)}) custom-call(bf16[64,1024]{1,0:T(8,128)(2,1)} %get-tuple-element.25.g_ref, f32[1,128]{1,0:T(1,128)} %get-tuple-element.26.live_ref), custom_call_target="tpu_custom_call" | custom-call | tf_op jit(solution)/shard_map/pallas_call | solution.py:292
  102.0 2.9 %fusion.1 = (f32[512]{0:T(512)S(1)}, bf16[512,1024]{1,0:T(8,128)(2,1)S(1)}, bf16[512,1024]{1,0:T(8,128)(2,1)}) fusion(f32[1024]{0:T(1024)S(1)} %bitcast.76, bf16[256,1024]{1,0:T(8,128)(2,1)} %bitcast.86, f32[512]{0:T(512)S(1)} %fusion.38, f32[256]{0:T(256)S(1)} %iota_convert_fusion, pred[512]{0:T(512)(128)(4,1)S(1)} %bitcast.81, ...), kind=kOutput, calls=%fused_computation.4 | convolution fusion | flops 272891392 | bytes 3679744 | tf_op jit(solution)/shard_map/dot_general | solution.py:415
  104.9 2.2 %copy-done.1 = bf16[2,1024,1024]{2,1,0:T(8,128)(2,1)S(1)} copy-done((bf16[2,1024,1024]{2,1,0:T(8,128)(2,1)S(1)}, bf16[2,1024,1024]{2,1,0:T(8,128)(2,1)}, u32[]{:S(2)}) %copy-start.1) | copy-done | bytes 4194328
  107.1 1.6 copy-done.6
  108.7 26.2 %shard_map.145 = (bf16[128,3584]{1,0:T(8,128)(2,1)S(1)}, f32[1,128]{1,0:T(1,128)S(1)}) custom-call(bf16[4,128,1024]{2,1,0:T(8,128)(2,1)S(1)} %bitcast.62, f32[4,1,128]{2,1,0:T(1,128)S(1)} %bitcast.64, bf16[2,1024,512]{2,1,0:T(8,128)(2,1)S(1)} %copy-done.2, bf16[2,1024,512]{2,1,0:T(8,128)(2,1)S(1)} %copy-done.4, bf16[2,1024,1024]{2,1,0:T(8,128)(2,1)S(1)} %copy-done.1, ...), custom_call_target="tpu_custom_call" | custom-call | tf_op jit(solution)/shard_map/pallas_call | solution.py:227
  136.6 10.2 %shard_map.146 = (bf16[128,1024]{1,0:T(8,128)(2,1)}, f32[2,16,4,128,256]{4,3,2,1,0:T(8,128)}) custom-call(bf16[128,3584]{1,0:T(8,128)(2,1)} %copy-done.7, f32[128,1]{1,0:T(8,128)} %copy.26.scale_ref, f32[128,1]{1,0:T(8,128)} %reshape.246.live_ref, f32[2,1,512]{2,1,0:T(1,128)} %reshape.217.bias_ref, ...), custom_call_target="tpu_custom_call", output_to_operand_aliasing={{1}: (7, {})} | custom-call | tf_op jit(solution)/shard_map/pallas_call | solution.py:373
  146.7 10.9 %shard_map.147 = (bf16[4,128,1024]{2,1,0:T(8,128)(2,1)}, f32[4,1,128]{2,1,0:T(1,128)}) custom-call(bf16[128,1024]{1,0:T(8,128)(2,1)} %get-tuple-element.31.g_ref, f32[1,128]{1,0:T(1,128)} %reshape.244.live_ref), custom_call_target="tpu_custom_call" | custom-call | tf_op jit(solution)/shard_map/pallas_call | solution.py:292
  159.8 3.8 %fusion.15 = bf16[256,1024]{1,0:T(8,128)(2,1)} fusion(bf16[2,1024,1024]{2,1,0:T(8,128)(2,1)} %param.24, bf16[512,1024]{1,0:T(8,128)(2,1)} %bitcast.84, f32[512]{0:T(512)S(1)} %fusion.37, f32[256]{0:T(256)S(1)} %iota_convert_fusion, pred[512]{0:T(512)(128)(4,1)S(1)} %bitcast.77), kind=kOutput, calls=%fused_computation.21 | convolution fusion | flops 806092800 | bytes 3673600 | tf_op jit(solution)/shard_map/dot_general | solution.py:409
  163.6 16.6 %shard_map.148 = (bf16[64,1024]{1,0:T(8,128)(2,1)}, f32[1,128]{1,0:T(1,128)}) custom-call(bf16[4,64,1024]{2,1,0:T(8,128)(2,1)} %bitcast.69, f32[4,1,128]{2,1,0:T(1,128)} %broadcast.78.ss_ref), custom_call_target="tpu_custom_call" | custom-call | tf_op jit(solution)/shard_map/pallas_call | solution.py:122
  180.2 11.8 %shard_map.149 = (bf16[4,64,1024]{2,1,0:T(8,128)(2,1)}, f32[4,1,128]{2,1,0:T(1,128)}) custom-call(bf16[64,1024]{1,0:T(8,128)(2,1)} %get-tuple-element.34.g_ref, f32[1,128]{1,0:T(1,128)} %get-tuple-element.35.live_ref), custom_call_target="tpu_custom_call" | custom-call | tf_op jit(solution)/shard_map/pallas_call | solution.py:292
  192.0 2.6 %fusion.11 = bf16[64,8,1024]{2,1,0:T(8,128)(2,1)} fusion(bf16[256,1024]{1,0:T(8,128)(2,1)} %bitcast.70, bf16[512,1024]{1,0:T(8,128)(2,1)S(1)} %copy-done.10, f32[512]{0:T(512)S(1)} %fusion.37, f32[256]{0:T(256)S(1)} %iota_convert_fusion, pred[512]{0:T(512)(128)(4,1)S(1)} %bitcast.78), kind=kOutput, calls=%fused_computation.17 | convolution fusion | flops 270270464 | bytes 2625024 | tf_op jit(solution)/shard_map/dot_general | solution.py:415
  (43 shorter events, 11.9 us)
Async XLA Ops:
  9.1 2.5 %copy-start = (bf16[2,1024,1024]{2,1,0:T(8,128)(2,1)S(1)}, bf16[2,1024,1024]{2,1,0:T(8,128)(2,1)}, u32[]{:S(2)}) copy-start(bf16[2,1024,1024]{2,1,0:T(8,128)(2,1)} %rest_2_.3) | copy-start | bytes 12582916
  10.7 1.8 copy-start.2
  12.5 1.6 copy-start.3
  14.1 1.6 copy-start.5
  43.3 0.9 copy-start.8
  69.1 32.9 %copy-start.9 = (bf16[64,8,1024]{2,1,0:T(8,128)(2,1)S(1)}, bf16[64,8,1024]{2,1,0:T(8,128)(2,1)}, u32[]{:S(2)}) copy-start(bf16[64,8,1024]{2,1,0:T(8,128)(2,1)} %param.13) | copy-start | bytes 3145732
  102.0 2.9 %copy-start.4 = (bf16[2,1024,512]{2,1,0:T(8,128)(2,1)S(1)}, bf16[2,1024,512]{2,1,0:T(8,128)(2,1)}, u32[]{:S(2)}) copy-start(bf16[2,1024,512]{2,1,0:T(8,128)(2,1)} %rest_1_.3) | copy-start | bytes 6291460
  104.9 2.2 %copy-start.1 = (bf16[2,1024,1024]{2,1,0:T(8,128)(2,1)S(1)}, bf16[2,1024,1024]{2,1,0:T(8,128)(2,1)}, u32[]{:S(2)}) copy-start(bf16[2,1024,1024]{2,1,0:T(8,128)(2,1)} %rest_2_.3) | copy-start | bytes 12582916
  107.1 1.6 copy-start.6
  134.9 0.9 copy-start.7
  159.8 32.2 %copy-start.10 = (bf16[512,1024]{1,0:T(8,128)(2,1)S(1)}, bf16[512,1024]{1,0:T(8,128)(2,1)}, u32[]{:S(2)}) copy-start(bf16[512,1024]{1,0:T(8,128)(2,1)} %get-tuple-element.42) | copy-start | bytes 3145732
